TPU v7x, 32 devices: a whole 2x2x4 slice. The times are simulated.
32 devices in a mesh: ep: 16 (over z, y, x), tp: 2 (over core).
Axes of the slice: x: 2, y: 2, z: 4, core: 2. Of those that a mesh axis runs over, the one named last changes fastest.
Arguments:
- tokens: bfloat16 [8192, 2048], P(('ep', 'tp')), may hold values from -6 to 6
- norm_gain: float32 [2048], replicated, may hold values from 0.1 to 1.9
- norm_bias: float32 [2048], replicated, may hold values from -3 to 3
- gate_weight: bfloat16 [16, 2048, 1024], P('ep', None, 'tp'), may hold values from -0.125 to 0.125
- up_weight: bfloat16 [16, 2048, 1024], P('ep', None, 'tp'), may hold values from -0.125 to 0.125
- down_weight: bfloat16 [16, 1024, 2048], P('ep', 'tp'), may hold values from -0.1875 to 0.1875
- expert_ids: int32 [8192, 2], P(('ep', 'tp')), may hold values from 0 to 15, all different within a row; in each aligned block of 256 rows (0 to 255, 256 to 511, ...) at most 64 rows name the same one
- route_weights: float32 [8192, 2], P(('ep', 'tp')), may hold values from 0.2 to 1
Outputs:
- mixed: bfloat16 [8192, 2048], P(('ep', 'tp'))
Inputs may be any that keep to these rules, and one draw needn't show every extreme that they name: `expert_ids`: a token's 2 experts differ; in the tokens of one device (aligned blocks of 256 rows) no expert is named by more than 64 entries, a bound that some block reaches.
All inputs are finite; a program needn't handle non-finite values.
Results may differ from a plain program's by a relative error of at most 0.0071.
Values may be sent and summed in bfloat16 or wider, within the bound.
A program may use at most 128 MiB of HBM per device.

v0:
```python
import jax
import jax.numpy as jnp
from jax import lax
from jax.sharding import PartitionSpec as P


def body(
    tokens, norm_gain, norm_bias, gate_weight, up_weight, down_weight, expert_ids, route_weights
):
    tok_rows, width = tokens.shape
    topk = expert_ids.shape[1]
    experts = lax.axis_size("ep")
    capacity = max(4 * tok_rows // experts, 4)
    values = tokens.astype(jnp.float32)
    centre = values - jnp.mean(values, axis=-1, keepdims=True)
    spread = jnp.mean(centre * centre, axis=-1, keepdims=True)
    normed = (centre * lax.rsqrt(spread + 1e-05) * norm_gain + norm_bias).astype(jnp.bfloat16)
    flat_ids = expert_ids.reshape(-1)
    onehot = (flat_ids[:, None] == jnp.arange(experts, dtype=jnp.int32)[None, :]).astype(jnp.int32)
    slot = jnp.sum(jnp.cumsum(onehot, axis=0) * onehot, axis=1) - 1
    target = flat_ids * capacity + slot
    buffer = (
        jnp.zeros((experts * capacity, width), jnp.bfloat16)
        .at[target]
        .set(jnp.repeat(normed, topk, axis=0))
    )
    buffer = buffer.reshape(experts, capacity, width)
    w_gate = gate_weight[0]
    w_up = up_weight[0]
    w_down = down_weight[0]
    rows = lax.all_to_all(buffer, "ep", split_axis=0, concat_axis=0, tiled=True)
    sources, slots, _ = rows.shape
    flat = rows.reshape(-1, width)
    pieces = lax.all_gather((w_gate, w_up), "tp", axis=1, tiled=True)
    gate = jnp.dot(flat, pieces[0], preferred_element_type=jnp.float32)
    upper = jnp.dot(flat, pieces[1], preferred_element_type=jnp.float32)
    hidden = (jax.nn.silu(gate) * upper).astype(jnp.bfloat16)
    result = jnp.dot(
        hidden, lax.all_gather(w_down, "tp", axis=0, tiled=True), preferred_element_type=jnp.float32
    ).astype(jnp.bfloat16)
    returned = lax.all_to_all(
        result.reshape(sources, slots, width), "ep", split_axis=0, concat_axis=0, tiled=True
    )
    picked = returned.reshape(-1, width)[target].astype(jnp.float32).reshape(tok_rows, topk, width)
    return jnp.sum(picked * route_weights[:, :, None], axis=1).astype(jnp.bfloat16)


def solution(mesh):
    placed = (
        P(("ep", "tp"), None),
        P(),
        P(),
        P("ep", None, "tp"),
        P("ep", None, "tp"),
        P("ep", "tp", None),
        P(("ep", "tp"), None),
        P(("ep", "tp"), None),
    )
    return jax.shard_map(
        body, mesh=mesh, in_specs=placed, out_specs=P(("ep", "tp"), None), check_vma=False
    )
```

profile of v0, /device:TPU:14, one launch (start us, length us, event | category | flops | bytes accessed | tf_op | source)
XLA Modules:
  0.0 279.5 jit_solution(123657268291948072)
XLA Ops:
  6.5 0.7 all-gather.9.cloned.1.call-update
  7.3 0.8 copy.11
  8.1 0.1 eq.29
  8.2 0.1 eq.25
  8.4 1.2 reduce-window.6
  9.5 0.2 slice_reduce_fusion
  9.8 0.7 broadcast_multiply_fusion
  10.5 0.1 copy.10
  10.6 0.1 mul.55
  10.8 1.4 convert_reduce_fusion
  12.2 0.4 fusion.13
  12.7 0.5 fusion.16
  13.2 1.3 broadcast_in_dim.5
  14.4 2.2 reshape.104
  16.7 0.1 fusion.20
  16.8 7.5 %scatter_custom_fusion = bf16[1024,2048]{1,0:T(8,128)(2,1)} fusion(s32[512]{0:T(512)S(1)} %bitcast.39, bf16[512,2048]{1,0:T(8,128)(2,1)} %reshape.104, bf16[]{:T(256)} %constant.9.clone.1), kind=kCustom, calls=%fused_computation.19 | custom fusion | bytes 4194816 | tf_op jit(solution)/shard_map/scatter | solution.py:25
  24.3 7.2 %all-to-all-start = ((bf16[16,64,2048]{2,1,0:T(8,128)(2,1)}), bf16[16,64,2048]{2,1,0:T(8,128)(2,1)}, u32[]{:S(2)}, u32[]{:S(2)}) async-start(bf16[16,64,2048]{2,1,0:T(8,128)(2,1)} %bitcast.37), calls=%async_computation | async-start | bytes 8388608 | tf_op jit(solution)/shard_map/all_to_all | solution.py:31
  31.5 0.0 all-gather.7.cloned.1.call-start
  31.5 0.7 all-gather.7.cloned.1.call-update
  32.2 0.2 all-gather.11.cloned.1.call-start
  32.4 0.5 all-gather.11.cloned.1.call-update
  33.0 0.0 all-gather.9.cloned.1.call-done
  33.0 93.2 %all-to-all-done = bf16[16,64,2048]{2,1,0:T(8,128)(2,1)} async-done(((bf16[16,64,2048]{2,1,0:T(8,128)(2,1)}), bf16[16,64,2048]{2,1,0:T(8,128)(2,1)}, u32[]{:S(2)}, u32[]{:S(2)}) %all-to-all-start) | async-done | bytes 4194336 | tf_op jit(solution)/shard_map/all_to_all | solution.py:31
  126.2 9.9 %fusion.2 = f32[1024,1024]{1,0:T(8,128)} fusion(bf16[1024,2048]{1,0:T(8,128)(2,1)} %bitcast.4, bf16[1,2048,1024]{2,1,0:T(8,128)(2,1)} %all-gather.9.cloned.1.call-done), kind=kOutput, calls=%fused_computation.4 | convolution fusion | flops 4294967296 | bytes 12582912 | tf_op jit(solution)/shard_map/dot_general | solution.py:36
  136.1 9.6 %multiply_convert_fusion = bf16[1024,1024]{1,0:T(8,128)(2,1)S(1)} fusion(f32[1024,1024]{1,0:T(8,128)} %fusion.2, bf16[1024,2048]{1,0:T(8,128)(2,1)} %bitcast.4, bf16[1,2048,1024]{2,1,0:T(8,128)(2,1)} %all-gather.7.cloned.1.call-done), kind=kOutput, calls=%fused_computation.9 | convolution fusion | flops 4301258752 | bytes 14680064 | tf_op jit(solution)/shard_map/dot_general | solution.py:35
  145.7 8.2 %fusion.6 = bf16[1024,2048]{1,0:T(8,128)(2,1)} fusion(bf16[1024,1024]{1,0:T(8,128)(2,1)S(1)} %multiply_convert_fusion, bf16[1,1024,2048]{2,1,0:T(8,128)(2,1)} %all-gather.11.cloned.1.call-done), kind=kOutput, calls=%fused_computation.10 | convolution fusion | flops 4297064448 | bytes 10485760 | tf_op jit(solution)/shard_map/dot_general | solution.py:38
  153.9 5.2 %all-to-all-start.1 = ((bf16[16,64,2048]{2,1,0:T(8,128)(2,1)}), bf16[16,64,2048]{2,1,0:T(8,128)(2,1)}, u32[]{:S(2)}, u32[]{:S(2)}) async-start(bf16[16,64,2048]{2,1,0:T(8,128)(2,1)} %bitcast.38), calls=%async_computation.1 | async-start | bytes 8388608 | tf_op jit(solution)/shard_map/all_to_all | solution.py:41
  159.2 0.1 copy.14
  159.3 92.7 %all-to-all-done.1 = bf16[16,64,2048]{2,1,0:T(8,128)(2,1)} async-done(((bf16[16,64,2048]{2,1,0:T(8,128)(2,1)}), bf16[16,64,2048]{2,1,0:T(8,128)(2,1)}, u32[]{:S(2)}, u32[]{:S(2)}) %all-to-all-start.1) | async-done | bytes 4194336 | tf_op jit(solution)/shard_map/all_to_all | solution.py:41
  252.0 7.1 %gather_fusion = bf16[512,2048]{1,0:T(8,128)(2,1)S(1)} fusion(bf16[1024,2048]{1,0:T(8,128)(2,1)} %bitcast.9, s32[1024]{0:T(1024)S(1)} %pad_clamp_fusion), kind=kCustom, calls=%fused_computation | custom fusion | bytes 4196352 | tf_op jit(solution)/shard_map/gather | solution.py:44
  259.1 4.0 %reshape.91 = f32[256,2,2048]{2,1,0:T(2,128)} reshape(bf16[512,2048]{1,0:T(8,128)(2,1)S(1)} %gather_fusion) | data formatting | bytes 6291456 | tf_op jit(solution)/shard_map/convert_element_type | solution.py:44
  263.1 9.9 %multiply_reduce_fusion = bf16[256,2048]{1,0:T(8,128)(2,1)} fusion(f32[256,2,2048]{2,1,0:T(2,128)} %reshape.91, f32[256,2]{1,0:T(8,128)S(1)} %copy.14), kind=kLoop, calls=%fused_computation.8 | loop fusion | flops 1572864 | bytes 5244928 | tf_op jit(solution)/shard_map/reduce_sum | solution.py:45
  (19 shorter events, 0.1 us)
Async XLA Ops:
  6.5 5.7 %copy-start = (bf16[256,2048]{1,0:T(8,128)(2,1)S(1)}, bf16[256,2048]{1,0:T(8,128)(2,1)}, u32[]{:S(2)}) copy-start(bf16[256,2048]{1,0:T(8,128)(2,1)} %param.8) | copy-start | bytes 3145732
  6.5 6.1 %copy-start.1 = (f32[2048]{0:T(1024)S(1)}, f32[2048]{0:T(1024)}, u32[]{:S(2)}) copy-start(f32[2048]{0:T(1024)} %param.10) | copy-start | bytes 24580
  6.5 6.1 %copy-start.2 = (f32[2048]{0:T(1024)S(1)}, f32[2048]{0:T(1024)}, u32[]{:S(2)}) copy-start(f32[2048]{0:T(1024)} %param.9) | copy-start | bytes 24580
  6.5 26.4 %all-gather.9.cloned.1.call-start = ((), (), s32[]{:S(2)}) async-start(), calls=%async_computation.3 | async-start | bytes 6291456 | tf_op jit(solution)/shard_map/all_gather | solution.py:34
  24.3 101.9 %all-to-all-start = ((bf16[16,64,2048]{2,1,0:T(8,128)(2,1)}), bf16[16,64,2048]{2,1,0:T(8,128)(2,1)}, u32[]{:S(2)}, u32[]{:S(2)}) async-start(bf16[16,64,2048]{2,1,0:T(8,128)(2,1)} %bitcast.37), calls=%async_computation | async-start | bytes 8388608 | tf_op jit(solution)/shard_map/all_to_all | solution.py:31
  31.5 104.6 %all-gather.7.cloned.1.call-start = ((), (), s32[]{:S(2)}) async-start(), calls=%async_computation.2 | async-start | bytes 6291456 | tf_op jit(solution)/shard_map/all_gather | solution.py:34
  32.2 113.4 %all-gather.11.cloned.1.call-start = ((), (), s32[]{:S(2)}) async-start(), calls=%async_computation.4 | async-start | bytes 6291456 | tf_op jit(solution)/shard_map/all_gather | solution.py:39
  153.9 5.3 %copy-start.3 = (f32[256,2]{0,1:T(2,128)S(1)}, f32[256,2]{0,1:T(2,128)}, u32[]{:S(2)}) copy-start(f32[256,2]{0,1:T(2,128)} %param.15) | copy-start | bytes 6148
  153.9 98.1 %all-to-all-start.1 = ((bf16[16,64,2048]{2,1,0:T(8,128)(2,1)}), bf16[16,64,2048]{2,1,0:T(8,128)(2,1)}, u32[]{:S(2)}, u32[]{:S(2)}) async-start(bf16[16,64,2048]{2,1,0:T(8,128)(2,1)} %bitcast.38), calls=%async_computation.1 | async-start | bytes 8388608 | tf_op jit(solution)/shard_map/all_to_all | solution.py:41
Sparse Core Ops, SparseCore 0:
  8.9 15.0 all-gather.8
  33.8 14.7 all-gather.6
  50.2 14.8 all-gather.10
where the time goes:
time: 280 us
  waiting for transfers between devices  188 us (67%)
  matrix products  27.7 us (10%)
  local copies, waits for them, and re-layouts  23.9 us (9%)
  other arithmetic  14.2 us (5%)
  between operations  13.2 us (5%)
  starting transfers between devices  12.7 us (5%)
    all_to_all x1, waiting for transfers between devices, body(): rows = lax.all_to_all(buffer, 'ep', split_axis=0, concat_axis=0, tiled=True)  93.2 us
    all_to_all x1, waiting for transfers between devices, body(): lax.all_to_all(result.reshape(sources, slots, width), 'ep', split_axis=0,...  92.7 us
    dot_general x1, matrix products, body(): upper = jnp.dot(flat, pieces[1], preferred_element_type=jnp.float32)  9.87 us
    reduce_sum x1, other arithmetic, body(): jnp.sum(picked * route_weights[:, :, None], axis=1).astype(jnp.bfloat16)  9.86 us
    dot_general x1, matrix products, body(): gate = jnp.dot(flat, pieces[0], preferred_element_type=jnp.float32)  9.55 us
    dot_general x1, matrix products, body(): jnp.dot(hidden, lax.all_gather(w_down, 'tp', axis=0, tiled=True), preferr...  8.22 us
    scatter x1, local copies, waits for them, and re-layouts, body(): buffer = jnp.zeros((experts * capacity, width), jnp.bfloat16).at[target]....  7.51 us
    all_to_all x1, starting transfers between devices, body(): rows = lax.all_to_all(buffer, 'ep', split_axis=0, concat_axis=0, tiled=True)  7.16 us
  transfers between devices with their start and end apart: 5, of which 2 were waited for; matrix products, arithmetic and copies ran while one was open for 13% of the time, Pallas kernels for 0%

commit v1 on v0

v1 whole, which is shorter than its diff:
```python
import functools

import jax
import jax.numpy as jnp
from jax import lax
from jax.experimental import pallas as pl
from jax.experimental.pallas import tpu as pltpu
from jax.sharding import PartitionSpec as P

MESH = pl.DeviceIdType.MESH
LINE = 4
CHUNKS = 8


def kernel(
    planes, nrm, meta, gw, uw, dw, out,
    tok, met, wg, wu, wd, sel, mix, snd, xin, hid, res, ret, psend, racc,
    s_own, s_met, s_mets, s_wl, s_ws, s_wr, s_tok, s_toks, s_x, s_xs, s_r, s_rs, s_p, s_ps,
):
    n = LINE
    side = planes
    me, core = lax.axis_index("ep"), lax.axis_index("tp")
    z, p = me // side, lax.rem(me, side)
    tokens, width = nrm.shape
    half = gw.shape[2]
    rows = snd.shape[1]
    cap = rows // side
    k = CHUNKS
    wide = width // k
    end = (z == 0) | (z == n - 1)
    mid = jnp.logical_not(end)
    step = jnp.where(z < n // 2, 1, -1)
    za, zb = z + step, z - step
    order = [
        z,
        jnp.where(end, z + 3 * step, z + 2 * step),
        jnp.where(end, z + 2 * step, z - step),
        z + step,
    ]

    def cols(c):
        return pl.ds(pl.multiple_of(c * wide, wide), wide)

    def band(i):
        return pl.ds(pl.multiple_of(i * cap, cap), cap)

    def plane(t):
        return {"ep": t * side + p}

    def peer(j):
        return lax.rem(p + j, side)

    def remote(src, dst, send, recv, where):
        return pltpu.make_async_remote_copy(
            src_ref=src, dst_ref=dst, send_sem=send, recv_sem=recv,
            device_id=where, device_id_type=MESH,
        )

    def landed(ref, sem):
        pltpu.make_async_copy(ref, ref, sem).wait()

    barrier = pltpu.get_barrier_semaphore()
    own = pltpu.make_async_copy(nrm, tok.at[z], s_own.at[0])
    own.start()
    ownm = pltpu.make_async_copy(meta, met.at[z], s_own.at[1])
    ownm.start()
    for j in range(1, side):
        pl.semaphore_signal(
            barrier, inc=1, device_id={"ep": z * side + peer(j)}, device_id_type=MESH
        )
    for j in range(1, n):
        pl.semaphore_signal(
            barrier, inc=1, device_id=plane(lax.rem(z + j, n)), device_id_type=MESH
        )
    pl.semaphore_signal(barrier, inc=1, device_id={"tp": 1 - core}, device_id_type=MESH)
    pl.semaphore_wait(barrier, side - 1 + n)

    def send_tok(s, c, to, way):
        remote(
            tok.at[s, :, cols(c)], tok.at[s, :, cols(c)],
            s_toks.at[way, s], s_tok.at[s, c], plane(to),
        ).start()

    def send_own(to, way):
        @pl.loop(0, k)
        def _(c):
            send_tok(z, c, to, way)

    own.wait()
    ownm.wait()
    for j in range(1, n):
        remote(
            met.at[z], met.at[z], s_mets.at[j - 1], s_met.at[z], plane(lax.rem(z + j, n))
        ).start()

    @pl.when(end)
    def _():
        send_own(za, 0)

    halfrows = pl.ds(pl.multiple_of(core * half, half), half)
    pairs = [
        (gw.at[0], wg.at[core]), (uw.at[0], wu.at[core]), (dw.at[0], wd.at[halfrows]),
    ]
    for i, (a, b) in enumerate(pairs):
        pltpu.make_async_copy(a, b, s_wl.at[i]).start()
        remote(a, b, s_ws.at[i], s_wr.at[i], {"tp": 1 - core}).start()

    def prep(q):
        s = order[q]
        ids0, ids1 = met[s, 0:1, :], met[s, 1:2, :]
        wt0, wt1 = met[s, 2:3, :], met[s, 3:4, :]
        row = lax.broadcasted_iota(jnp.int32, (rows, tokens), 0)
        e_row = (z * side + row // cap).astype(jnp.float32)
        s_row = lax.rem(row, cap).astype(jnp.float32)
        hit0 = (ids0 == e_row).astype(jnp.float32)
        hit1 = (ids1 == e_row).astype(jnp.float32)
        hit = hit0 + hit1
        before = (
            lax.broadcasted_iota(jnp.int32, (tokens, tokens), 0)
            < lax.broadcasted_iota(jnp.int32, (tokens, tokens), 1)
        ).astype(jnp.float32).astype(jnp.bfloat16)
        count = jnp.dot(hit.astype(jnp.bfloat16), before, preferred_element_type=jnp.float32)
        pick = jnp.where(count == s_row, hit, 0.0)
        sel[q] = pick.astype(jnp.bfloat16)
        w = pick * (hit0 * wt0 + hit1 * wt1)
        high = w.astype(jnp.bfloat16)
        mix[q, 0] = high
        mix[q, 1] = (w - high.astype(jnp.float32)).astype(jnp.bfloat16)

    def disp(q, c):
        y = jnp.dot(sel[q], tok[order[q], :, cols(c)], preferred_element_type=jnp.float32)
        snd[q, :, cols(c)] = y.astype(jnp.bfloat16)
        xin[q, band(p), cols(c)] = snd[q, band(p), cols(c)]
        for j in range(1, side):
            o = peer(j)
            remote(
                snd.at[q, band(o), cols(c)], xin.at[q, band(p), cols(c)],
                s_xs.at[q], s_x.at[q], {"ep": z * side + o},
            ).start()

    def others(ref, q):
        return ref.at[q, pl.ds(0, (side - 1) * cap)]

    tile = min(256, half)
    per = half // tile

    def compute(q):
        landed(others(xin, q), s_x.at[q])

        @pl.loop(0, 2 * per)
        def _(i):
            h, at = i // per, lax.rem(i, per)
            part = pl.ds(pl.multiple_of(at * tile, tile), tile)
            x = xin[q]
            g = jnp.dot(x, wg[h, :, part], preferred_element_type=jnp.float32)
            u = jnp.dot(x, wu[h, :, part], preferred_element_type=jnp.float32)
            v = g / (1.0 + jnp.exp(-g)) * u
            hid[:, pl.ds(pl.multiple_of(i * tile, tile), tile)] = v.astype(jnp.bfloat16)

        @pl.loop(0, k)
        def _(c):
            y = jnp.dot(hid[...], wd[:, cols(c)], preferred_element_type=jnp.float32)
            res[q, :, cols(c)] = y.astype(jnp.bfloat16)
            ret[q, band(p), cols(c)] = res[q, band(p), cols(c)]
            for j in range(1, side):
                o = peer(j)
                remote(
                    res.at[q, band(o), cols(c)], ret.at[q, band(p), cols(c)],
                    s_rs.at[q], s_r.at[q, c], {"ep": z * side + o},
                ).start()

    def weigh(q, c):
        landed(ret.at[q, pl.ds(0, (side - 1) * cap), cols(c)], s_r.at[q, c])
        r = ret[q, :, cols(c)]
        dims = (((0,), (0,)), ((), ()))
        return lax.dot_general(
            mix[q, 0], r, dims, preferred_element_type=jnp.float32
        ) + lax.dot_general(mix[q, 1], r, dims, preferred_element_type=jnp.float32)

    def combine(q, c, add):
        t = order[q]
        y = weigh(q, c)
        to = zb if (q == 2 and add) else za
        if add:
            landed(racc.at[t, c], s_p.at[t, c])
            y = y + racc[t, c].astype(jnp.float32)
        psend[q - 1, c] = y.astype(jnp.bfloat16)
        slot = jnp.where((to == t) & (to < z), n, t)
        remote(
            psend.at[q - 1, c], racc.at[slot, c], s_ps.at[q - 1], s_p.at[slot, c], plane(to)
        ).start()

    def arrived(s, c):
        landed(tok.at[s, :, cols(c)], s_tok.at[s, c])

    prep(0)

    @pl.loop(0, k)
    def _(c):
        disp(0, c)

    for q in range(1, n):
        landed(met.at[order[q]], s_met.at[order[q]])
        prep(q)

    def first(c):
        @pl.when(mid)
        def _():
            arrived(order[2], c)
            send_tok(order[2], c, za, 0)

        arrived(order[1], c)

        @pl.when(mid)
        def _():
            send_tok(order[1], c, zb, 1)

        disp(1, c)

        @pl.when(mid)
        def _():
            disp(2, c)

    pl.loop(0, k - 2)(first)
    for i, (a, b) in enumerate(pairs):
        pltpu.make_async_copy(a, b, s_wl.at[i]).wait()
        landed(b, s_wr.at[i])
    compute(0)
    pl.loop(k - 2, k)(first)

    @pl.when(mid)
    def _():
        send_own(za, 0)

    def second(c):
        @pl.when(mid)
        def _():
            arrived(order[3], c)
            send_tok(order[3], c, zb, 1)
            disp(3, c)

        @pl.when(end)
        def _():
            arrived(order[2], c)
            disp(2, c)

    pl.loop(0, k // 2)(second)
    compute(1)
    pl.loop(k // 2, k)(second)

    @pl.when(mid)
    def _():
        send_own(zb, 1)

    @pl.when(end)
    def _():
        pl.loop(0, k)(lambda c: combine(1, c, False))

    compute(2)

    @pl.when(end)
    def _():
        pl.loop(0, k)(lambda c: combine(2, c, False))

        @pl.loop(0, k)
        def _(c):
            arrived(order[3], c)
            disp(3, c)

    compute(3)

    @pl.when(mid)
    def _():
        @pl.loop(0, k)
        def _(c):
            combine(1, c, True)
            combine(2, c, True)

        pl.loop(0, k)(lambda c: combine(3, c, True))

    @pl.when(end)
    def _():
        pl.loop(0, k)(lambda c: combine(3, c, False))

    def last(c, slots):
        y = weigh(0, c)
        for slot in slots:
            landed(racc.at[slot, c], s_p.at[slot, c])
            y = y + racc[slot, c].astype(jnp.float32)
        out[:, cols(c)] = y.astype(out.dtype)

    @pl.when(end)
    def _():
        pl.loop(0, k)(lambda c: last(c, [jnp.where(z == 0, n, z)]))

    @pl.when(mid)
    def _():
        pl.loop(0, k)(lambda c: last(c, [z, n]))

    drain = landed

    for j in range(1, n):
        drain(met.at[z], s_mets.at[j - 1])
    for i, (a, b) in enumerate(pairs):
        drain(b, s_ws.at[i])
    drain(tok.at[z], s_toks.at[0, z])

    @pl.when(mid)
    def _():
        drain(tok.at[z], s_toks.at[1, z])
        drain(tok.at[z], s_toks.at[0, order[2]])
        drain(tok.at[z], s_toks.at[1, order[1]])
        drain(tok.at[z], s_toks.at[1, order[3]])

    for q in range(n):
        drain(others(snd, q), s_xs.at[q])
        drain(others(res, q), s_rs.at[q])
    for q in range(1, n):
        drain(psend.at[q - 1], s_ps.at[q - 1])


def body(
    tokens, norm_gain, norm_bias, gate_weight, up_weight, down_weight, expert_ids, route_weights
):
    count, width = tokens.shape
    experts = lax.axis_size("ep")
    cap = max(4 * count // experts, 4)
    side = experts // LINE
    half = gate_weight.shape[2]
    values = tokens.astype(jnp.float32)
    centre = values - jnp.mean(values, axis=-1, keepdims=True)
    spread = jnp.mean(centre * centre, axis=-1, keepdims=True)
    normed = (centre * lax.rsqrt(spread + 1e-05) * norm_gain + norm_bias).astype(jnp.bfloat16)
    both = jnp.concatenate([expert_ids.astype(jnp.float32), route_weights], axis=1)
    meta = jnp.pad(both.T, ((0, 4), (0, 0)))
    rows = side * cap
    wide = width // CHUNKS
    bf = jnp.bfloat16
    dma = pltpu.SemaphoreType.DMA
    hbm = pl.BlockSpec(memory_space=pl.ANY)
    return pl.pallas_call(
        functools.partial(kernel, side),
        out_shape=jax.ShapeDtypeStruct((count, width), bf),
        in_specs=[hbm] * 5,
        out_specs=pl.BlockSpec(memory_space=pltpu.VMEM),
        scratch_shapes=[
            pltpu.VMEM((LINE, count, width), bf),
            pltpu.VMEM((LINE, 8, count), jnp.float32),
            pltpu.VMEM((2, width, half), bf),
            pltpu.VMEM((2, width, half), bf),
            pltpu.VMEM((2 * half, width), bf),
            pltpu.VMEM((LINE, rows, count), bf),
            pltpu.VMEM((LINE, 2, rows, count), bf),
            pltpu.VMEM((LINE, rows, width), bf),
            pltpu.VMEM((LINE, rows, width), bf),
            pltpu.VMEM((rows, 2 * half), bf),
            pltpu.VMEM((LINE, rows, width), bf),
            pltpu.VMEM((LINE, rows, width), bf),
            pltpu.VMEM((LINE - 1, CHUNKS, count, wide), bf),
            pltpu.VMEM((LINE + 1, CHUNKS, count, wide), bf),
            dma((2,)),
            dma((LINE,)),
            dma((LINE - 1,)),
            dma((3,)),
            dma((3,)),
            dma((3,)),
            dma((LINE, CHUNKS)),
            dma((2, LINE)),
            dma((LINE,)),
            dma((LINE,)),
            dma((LINE, CHUNKS)),
            dma((LINE,)),
            dma((LINE + 1, CHUNKS)),
            dma((LINE - 1,)),
        ],
        compiler_params=pltpu.CompilerParams(
            collective_id=0, has_side_effects=True, vmem_limit_bytes=60 * 1024 * 1024
        ),
    )(normed, meta, gate_weight, up_weight, down_weight)


def solution(mesh):
    placed = (
        P(("ep", "tp"), None),
        P(),
        P(),
        P("ep", None, "tp"),
        P("ep", None, "tp"),
        P("ep", "tp", None),
        P(("ep", "tp"), None),
        P(("ep", "tp"), None),
    )
    return jax.shard_map(
        body, mesh=mesh, in_specs=placed, out_specs=P(("ep", "tp"), None), check_vma=False
    )
```

time: 280 us -> 161 us (0.57)
  waiting for transfers between devices: 188 us -> 0 us
  Pallas kernels: 0 us -> 152 us
  matrix products: 27.7 us -> 0 us
  local copies, waits for them, and re-layouts: 23.9 us -> 2.92 us
  between operations: 13.2 us -> 0.07 us
  starting transfers between devices: 12.7 us -> 0 us
  other arithmetic: 14.2 us -> 4.63 us
    all_to_all x2 -> x0, waiting for transfers between devices: 186 us -> none  [the longest x1 93.2 us: body(): rows = lax.all_to_all(buffer, 'ep', split_axis=0, concat_axis=0, tiled=True)]
    pallas_call x0 -> x1, Pallas kernels: none -> 152 us  [body(): pl.pallas_call(functools.partial(kernel, side), out_shape=jax.ShapeDtypeS...]
    dot_general x3 -> x0, matrix products: 27.7 us -> none  [the longest x1 9.87 us: body(): upper = jnp.dot(flat, pieces[1], preferred_element_type=jnp.float32)]
    all_to_all x2 -> x0, starting transfers between devices: 12.4 us -> none  [the longest x1 7.16 us: body(): rows = lax.all_to_all(buffer, 'ep', split_axis=0, concat_axis=0, tiled=True)]
    reduce_sum x2 -> x0, other arithmetic: 9.95 us -> none  [the longest x1 9.86 us: body(): jnp.sum(picked * route_weights[:, :, None], axis=1).astype(jnp.bfloat16)]
    scatter x1 -> x0, local copies, waits for them, and re-layouts: 7.51 us -> none  [body(): buffer = jnp.zeros((experts * capacity, width), jnp.bfloat16).at[target]....]
    gather x1 -> x0, local copies, waits for them, and re-layouts: 7.13 us -> none  [body(): returned.reshape(-1, width)[target].astype(jnp.float32)]
    convert_element_type x1 -> x0, local copies, waits for them, and re-layouts: 4 us -> none  [body(): returned.reshape(-1, width)[target].astype(jnp.float32)]
  transfers between devices with their start and end apart: 5 -> 0, of which waited for: 2 -> 0; matrix products, arithmetic and copies ran while one was open for 13% -> 0% of each run, Pallas kernels for 0% -> 0%
where the time goes in v1:
time: 161 us; the launch traced here: 160 us
  Pallas kernels  152 us (94%)
  other arithmetic  4.63 us (3%)
  local copies, waits for them, and re-layouts  2.92 us (2%)
    pallas_call x1, Pallas kernels, body(): pl.pallas_call(functools.partial(kernel, side), out_shape=jax.ShapeDtypeS...  152 us

profile of v1, /device:TPU:14, one launch (start us, length us, event | category | flops | bytes accessed | tf_op | source)
XLA Modules:
  0.0 160.0 jit_solution(5523121022664958700)
XLA Ops:
  0.0 0.0 copy-start
  0.0 0.0 copy-start.4
  0.0 0.0 copy-start.3
  0.0 0.0 copy-start.1
  0.0 0.0 copy-start.2
  0.0 1.5 convert_reduce_fusion
  1.6 1.6 %fusion.2 = f32[256]{0:T(256)S(1)} fusion(bf16[256,2048]{1,0:T(8,128)(2,1)} %param.8, f32[256]{0:T(256)S(1)} %broadcast_multiply_fusion), kind=kLoop, calls=%fused_computation.4 | loop fusion | flops 2096896 | bytes 1050624 | tf_op jit(solution)/shard_map/reduce_sum | solution.py:332
  3.2 0.0 copy-done.3
  3.2 0.0 copy-done.4
  3.3 0.6 pad.4.meta
  3.9 0.0 copy-done
  3.9 0.0 copy-done.1
  3.9 0.0 copy-done.2
  3.9 1.4 fusion.5.nrm
  5.3 152.4 %shard_map.82 = bf16[256,2048]{1,0:T(8,128)(2,1)} custom-call(bf16[256,2048]{1,0:T(8,128)(2,1)} %fusion.5.nrm, f32[8,256]{1,0:T(8,128)} %pad.4.meta, bf16[1,2048,512]{2,1,0:T(8,128)(2,1)} %gw.1, bf16[1,2048,512]{2,1,0:T(8,128)(2,1)} %uw.1, bf16[1,512,2048]{2,1,0:T(8,128)(2,1)} %dw.1), custom_call_target="tpu_custom_call" | custom-call | tf_op jit(solution)/shard_map/pallas_call | solution.py:341
  157.7 2.3 %copy.10 = bf16[256,2048]{1,0:T(8,128)(2,1)} copy(bf16[256,2048]{1,0:T(8,128)(2,1)} %shard_map.82) | data formatting | bytes 2097152
  (4 shorter events, 0.0 us)
Async XLA Ops:
  0.0 3.9 %copy-start = (bf16[256,2048]{1,0:T(8,128)(2,1)S(1)}, bf16[256,2048]{1,0:T(8,128)(2,1)}, u32[]{:S(2)}) copy-start(bf16[256,2048]{1,0:T(8,128)(2,1)} %param.8) | copy-start | bytes 3145732
  0.0 3.2 %copy-start.4 = (f32[256,2]{0,1:T(2,128)S(1)}, f32[256,2]{0,1:T(2,128)}, u32[]{:S(2)}) copy-start(f32[256,2]{0,1:T(2,128)} %param.15) | copy-start | bytes 6148
  0.0 3.2 %copy-start.3 = (s32[256,2]{0,1:T(2,128)S(1)}, s32[256,2]{0,1:T(2,128)}, u32[]{:S(2)}) copy-start(s32[256,2]{0,1:T(2,128)} %param.14) | copy-start | bytes 6148
  0.0 3.9 %copy-start.1 = (f32[2048]{0:T(1024)S(1)}, f32[2048]{0:T(1024)}, u32[]{:S(2)}) copy-start(f32[2048]{0:T(1024)} %param.10) | copy-start | bytes 24580
  0.0 3.9 %copy-start.2 = (f32[2048]{0:T(1024)S(1)}, f32[2048]{0:T(1024)}, u32[]{:S(2)}) copy-start(f32[2048]{0:T(1024)} %param.9) | copy-start | bytes 24580

commit v2 on v1

--- a/solution.py
+++ b/solution.py
@@ -10,6 +10,7 @@
 MESH = pl.DeviceIdType.MESH
 LINE = 4
 CHUNKS = 8
+LAG = 2
 
 
 def kernel(
@@ -203,12 +204,14 @@
         landed(met.at[order[q]], s_met.at[order[q]])
         prep(q)
 
-    def first(c):
+    def near(c):
         @pl.when(mid)
         def _():
             arrived(order[2], c)
             send_tok(order[2], c, za, 0)
-
+            disp(2, c)
+
+    def far(c):
         arrived(order[1], c)
 
         @pl.when(mid)
@@ -217,20 +220,23 @@
 
         disp(1, c)
 
-        @pl.when(mid)
-        def _():
-            disp(2, c)
-
-    pl.loop(0, k - 2)(first)
+    for c in range(LAG):
+        near(c)
+
+    @pl.loop(LAG, k)
+    def _(c):
+        near(c)
+        far(c - LAG)
+
+    @pl.when(mid)
+    def _():
+        send_own(za, 0)
+
     for i, (a, b) in enumerate(pairs):
         pltpu.make_async_copy(a, b, s_wl.at[i]).wait()
         landed(b, s_wr.at[i])
     compute(0)
-    pl.loop(k - 2, k)(first)
-
-    @pl.when(mid)
-    def _():
-        send_own(za, 0)
+    pl.loop(k - LAG, k)(far)
 
     def second(c):
         @pl.when(mid)
@@ -260,10 +266,9 @@
 
     @pl.when(end)
     def _():
-        pl.loop(0, k)(lambda c: combine(2, c, False))
-
         @pl.loop(0, k)
         def _(c):
+            combine(2, c, False)
             arrived(order[3], c)
             disp(3, c)
 
@@ -271,11 +276,15 @@
 
     @pl.when(mid)
     def _():
-        @pl.loop(0, k)
+        for c in range(LAG):
+            combine(1, c, True)
+
+        @pl.loop(LAG, k)
         def _(c):
             combine(1, c, True)
-            combine(2, c, True)
-
+            combine(2, c - LAG, True)
+
+        pl.loop(k - LAG, k)(lambda c: combine(2, c, True))
         pl.loop(0, k)(lambda c: combine(3, c, True))
 
     @pl.when(end)

time: 161 us -> 145 us (0.901)
  Pallas kernels: 152 us -> 135 us
    pallas_call x1, Pallas kernels: 152 us -> 135 us  [body(): pl.pallas_call(functools.partial(kernel, side), out_shape=jax.ShapeDtypeS...]
where the time goes in v2:
time: 145 us; the launch traced here: 143 us
  Pallas kernels  135 us (93%)
  other arithmetic  4.63 us (3%)
  local copies, waits for them, and re-layouts  2.92 us (2%)
    pallas_call x1, Pallas kernels, body(): pl.pallas_call(functools.partial(kernel, side), out_shape=jax.ShapeDtypeS...  135 us

profile of v2, /device:TPU:14, one launch (start us, length us, event | category | flops | bytes accessed | tf_op | source)
XLA Modules:
  0.0 142.9 jit_solution(2741033529398106970)
XLA Ops:
  0.0 0.0 copy-start
  0.0 0.0 copy-start.4
  0.0 0.0 copy-start.3
  0.0 0.0 copy-start.1
  0.0 0.0 copy-start.2
  0.0 1.5 %convert_reduce_fusion = f32[256]{0:T(256)S(1)} fusion(bf16[256,2048]{1,0:T(8,128)(2,1)} %param.8), kind=kLoop, calls=%fused_computation.1 | loop fusion | flops 1048320 | bytes 1049600 | tf_op jit(solution)/shard_map/reduce_sum | solution.py:340
  1.6 1.6 %fusion.2 = f32[256]{0:T(256)S(1)} fusion(bf16[256,2048]{1,0:T(8,128)(2,1)} %param.8, f32[256]{0:T(256)S(1)} %broadcast_multiply_fusion), kind=kLoop, calls=%fused_computation.4 | loop fusion | flops 2096896 | bytes 1050624 | tf_op jit(solution)/shard_map/reduce_sum | solution.py:341
  3.2 0.0 copy-done.3
  3.2 0.0 copy-done.4
  3.3 0.6 pad.4.meta
  3.9 0.0 copy-done
  3.9 0.0 copy-done.1
  3.9 0.0 copy-done.2
  3.9 1.4 %fusion.5.nrm = bf16[256,2048]{1,0:T(8,128)(2,1)} fusion(bf16[256,2048]{1,0:T(8,128)(2,1)S(1)} %copy-done, f32[2048]{0:T(1024)S(1)} %copy-done.1, f32[2048]{0:T(1024)S(1)} %copy-done.2, f32[256]{0:T(256)S(1)} %add_rsqrt_fusion, f32[256]{0:T(256)S(1)} %broadcast_multiply_fusion), kind=kLoop, calls=%fused_computation.7 | loop fusion | flops 3145728 | bytes 2115584 | tf_op jit(solution)/shard_map/convert_element_type | solution.py:342
  5.3 135.3 %shard_map.82 = bf16[256,2048]{1,0:T(8,128)(2,1)} custom-call(bf16[256,2048]{1,0:T(8,128)(2,1)} %fusion.5.nrm, f32[8,256]{1,0:T(8,128)} %pad.4.meta, bf16[1,2048,512]{2,1,0:T(8,128)(2,1)} %gw.1, bf16[1,2048,512]{2,1,0:T(8,128)(2,1)} %uw.1, bf16[1,512,2048]{2,1,0:T(8,128)(2,1)} %dw.1), custom_call_target="tpu_custom_call" | custom-call | tf_op jit(solution)/shard_map/pallas_call | solution.py:350
  140.6 2.3 %copy.10 = bf16[256,2048]{1,0:T(8,128)(2,1)} copy(bf16[256,2048]{1,0:T(8,128)(2,1)} %shard_map.82) | data formatting | bytes 2097152
  (4 shorter events, 0.0 us)
Async XLA Ops:
  0.0 3.9 %copy-start = (bf16[256,2048]{1,0:T(8,128)(2,1)S(1)}, bf16[256,2048]{1,0:T(8,128)(2,1)}, u32[]{:S(2)}) copy-start(bf16[256,2048]{1,0:T(8,128)(2,1)} %param.8) | copy-start | bytes 3145732
  0.0 3.2 %copy-start.4 = (f32[256,2]{0,1:T(2,128)S(1)}, f32[256,2]{0,1:T(2,128)}, u32[]{:S(2)}) copy-start(f32[256,2]{0,1:T(2,128)} %param.15) | copy-start | bytes 6148
  0.0 3.2 %copy-start.3 = (s32[256,2]{0,1:T(2,128)S(1)}, s32[256,2]{0,1:T(2,128)}, u32[]{:S(2)}) copy-start(s32[256,2]{0,1:T(2,128)} %param.14) | copy-start | bytes 6148
  0.0 3.9 %copy-start.1 = (f32[2048]{0:T(1024)S(1)}, f32[2048]{0:T(1024)}, u32[]{:S(2)}) copy-start(f32[2048]{0:T(1024)} %param.10) | copy-start | bytes 24580
  0.0 3.9 %copy-start.2 = (f32[2048]{0:T(1024)S(1)}, f32[2048]{0:T(1024)}, u32[]{:S(2)}) copy-start(f32[2048]{0:T(1024)} %param.9) | copy-start | bytes 24580

commit v3 on v2

--- a/solution.py
+++ b/solution.py
@@ -145,19 +145,16 @@
     tile = min(256, half)
     per = half // tile
 
-    def compute(q):
-        landed(others(xin, q), s_x.at[q])
-
-        @pl.loop(0, 2 * per)
-        def _(i):
-            h, at = i // per, lax.rem(i, per)
-            part = pl.ds(pl.multiple_of(at * tile, tile), tile)
-            x = xin[q]
-            g = jnp.dot(x, wg[h, :, part], preferred_element_type=jnp.float32)
-            u = jnp.dot(x, wu[h, :, part], preferred_element_type=jnp.float32)
-            v = g / (1.0 + jnp.exp(-g)) * u
-            hid[:, pl.ds(pl.multiple_of(i * tile, tile), tile)] = v.astype(jnp.bfloat16)
-
+    def gate(q, i):
+        h, at = i // per, lax.rem(i, per)
+        part = pl.ds(pl.multiple_of(at * tile, tile), tile)
+        x = xin[q]
+        g = jnp.dot(x, wg[h, :, part], preferred_element_type=jnp.float32)
+        u = jnp.dot(x, wu[h, :, part], preferred_element_type=jnp.float32)
+        v = g / (1.0 + jnp.exp(-g)) * u
+        hid[:, pl.ds(pl.multiple_of(i * tile, tile), tile)] = v.astype(jnp.bfloat16)
+
+    def down(q):
         @pl.loop(0, k)
         def _(c):
             y = jnp.dot(hid[...], wd[:, cols(c)], preferred_element_type=jnp.float32)
@@ -169,6 +166,11 @@
                     res.at[q, band(o), cols(c)], ret.at[q, band(p), cols(c)],
                     s_rs.at[q], s_r.at[q, c], {"ep": z * side + o},
                 ).start()
+
+    def compute(q):
+        landed(others(xin, q), s_x.at[q])
+        pl.loop(0, 2 * per)(lambda i: gate(q, i))
+        down(q)
 
     def weigh(q, c):
         landed(ret.at[q, pl.ds(0, (side - 1) * cap), cols(c)], s_r.at[q, c])
@@ -232,63 +234,62 @@
     def _():
         send_own(za, 0)
 
+    pl.loop(k - LAG, k)(far)
+
     for i, (a, b) in enumerate(pairs):
         pltpu.make_async_copy(a, b, s_wl.at[i]).wait()
         landed(b, s_wr.at[i])
-    compute(0)
-    pl.loop(k - LAG, k)(far)
-
-    def second(c):
-        @pl.when(mid)
-        def _():
+
+    @pl.when(mid)
+    def _():
+        def pass_on(c):
             arrived(order[3], c)
             send_tok(order[3], c, zb, 1)
             disp(3, c)
 
-        @pl.when(end)
-        def _():
+        pl.loop(0, k // 2)(pass_on)
+        landed(others(xin, 1), s_x.at[1])
+        turns = k - k // 2
+        for j in range(turns):
+            pass_on(k // 2 + j)
+            for i in range(j * 2 * per // turns, (j + 1) * 2 * per // turns):
+                gate(1, i)
+        send_own(zb, 1)
+        down(1)
+        compute(2)
+        compute(3)
+        for c in range(LAG):
+            combine(1, c, True)
+
+        @pl.loop(LAG, k)
+        def _(c):
+            combine(1, c, True)
+            combine(2, c - LAG, True)
+
+        pl.loop(k - LAG, k)(lambda c: combine(2, c, True))
+        compute(0)
+        pl.loop(0, k)(lambda c: combine(3, c, True))
+
+    @pl.when(end)
+    def _():
+        compute(1)
+
+        @pl.loop(0, k)
+        def _(c):
             arrived(order[2], c)
             disp(2, c)
-
-    pl.loop(0, k // 2)(second)
-    compute(1)
-    pl.loop(k // 2, k)(second)
-
-    @pl.when(mid)
-    def _():
-        send_own(zb, 1)
-
-    @pl.when(end)
-    def _():
-        pl.loop(0, k)(lambda c: combine(1, c, False))
-
-    compute(2)
-
-    @pl.when(end)
-    def _():
+            combine(1, c, False)
+
+        compute(0)
+        compute(2)
+
         @pl.loop(0, k)
         def _(c):
             combine(2, c, False)
             arrived(order[3], c)
             disp(3, c)
 
-    compute(3)
-
-    @pl.when(mid)
-    def _():
-        for c in range(LAG):
-            combine(1, c, True)
-
-        @pl.loop(LAG, k)
-        def _(c):
-            combine(1, c, True)
-            combine(2, c - LAG, True)
-
-        pl.loop(k - LAG, k)(lambda c: combine(2, c, True))
-        pl.loop(0, k)(lambda c: combine(3, c, True))
-
-    @pl.when(end)
-    def _():
+        compute(3)
         pl.loop(0, k)(lambda c: combine(3, c, False))
 
     def last(c, slots):

time: 145 us -> 141 us (0.972)
  Pallas kernels: 135 us -> 132 us
    pallas_call x1, Pallas kernels: 135 us -> 132 us  [body(): pl.pallas_call(functools.partial(kernel, side), out_shape=jax.ShapeDtypeS...]
where the time goes in v3:
time: 141 us; the launch traced here: 139 us
  Pallas kernels  132 us (94%)
  other arithmetic  4.63 us (3%)
  local copies, waits for them, and re-layouts  2.92 us (2%)
    pallas_call x1, Pallas kernels, body(): pl.pallas_call(functools.partial(kernel, side), out_shape=jax.ShapeDtypeS...  132 us

profile of v3, /device:TPU:14, one launch (start us, length us, event | category | flops | bytes accessed | tf_op | source)
XLA Modules:
  0.0 139.4 jit_solution(9495951112228975999)
XLA Ops:
  0.0 0.0 copy-start
  0.0 0.0 copy-start.4
  0.0 0.0 copy-start.3
  0.0 0.0 copy-start.1
  0.0 0.0 copy-start.2
  0.0 1.5 %convert_reduce_fusion = f32[256]{0:T(256)S(1)} fusion(bf16[256,2048]{1,0:T(8,128)(2,1)} %param.8), kind=kLoop, calls=%fused_computation.1 | loop fusion | flops 1048320 | bytes 1049600 | tf_op jit(solution)/shard_map/reduce_sum | solution.py:341
  1.6 1.6 %fusion.2 = f32[256]{0:T(256)S(1)} fusion(bf16[256,2048]{1,0:T(8,128)(2,1)} %param.8, f32[256]{0:T(256)S(1)} %broadcast_multiply_fusion), kind=kLoop, calls=%fused_computation.4 | loop fusion | flops 2096896 | bytes 1050624 | tf_op jit(solution)/shard_map/reduce_sum | solution.py:342
  3.2 0.0 copy-done.3
  3.2 0.0 copy-done.4
  3.3 0.6 pad.4.meta
  3.9 0.0 copy-done
  3.9 0.0 copy-done.1
  3.9 0.0 copy-done.2
  3.9 1.4 %fusion.5.nrm = bf16[256,2048]{1,0:T(8,128)(2,1)} fusion(bf16[256,2048]{1,0:T(8,128)(2,1)S(1)} %copy-done, f32[2048]{0:T(1024)S(1)} %copy-done.1, f32[2048]{0:T(1024)S(1)} %copy-done.2, f32[256]{0:T(256)S(1)} %add_rsqrt_fusion, f32[256]{0:T(256)S(1)} %broadcast_multiply_fusion), kind=kLoop, calls=%fused_computation.7 | loop fusion | flops 3145728 | bytes 2115584 | tf_op jit(solution)/shard_map/convert_element_type | solution.py:343
  5.3 131.7 %shard_map.82 = bf16[256,2048]{1,0:T(8,128)(2,1)} custom-call(bf16[256,2048]{1,0:T(8,128)(2,1)} %fusion.5.nrm, f32[8,256]{1,0:T(8,128)} %pad.4.meta, bf16[1,2048,512]{2,1,0:T(8,128)(2,1)} %gw.1, bf16[1,2048,512]{2,1,0:T(8,128)(2,1)} %uw.1, bf16[1,512,2048]{2,1,0:T(8,128)(2,1)} %dw.1), custom_call_target="tpu_custom_call" | custom-call | tf_op jit(solution)/shard_map/pallas_call | solution.py:351
  137.1 2.3 %copy.10 = bf16[256,2048]{1,0:T(8,128)(2,1)} copy(bf16[256,2048]{1,0:T(8,128)(2,1)} %shard_map.82) | data formatting | bytes 2097152
  (4 shorter events, 0.0 us)
Async XLA Ops:
  0.0 3.9 %copy-start = (bf16[256,2048]{1,0:T(8,128)(2,1)S(1)}, bf16[256,2048]{1,0:T(8,128)(2,1)}, u32[]{:S(2)}) copy-start(bf16[256,2048]{1,0:T(8,128)(2,1)} %param.8) | copy-start | bytes 3145732
  0.0 3.2 %copy-start.4 = (f32[256,2]{0,1:T(2,128)S(1)}, f32[256,2]{0,1:T(2,128)}, u32[]{:S(2)}) copy-start(f32[256,2]{0,1:T(2,128)} %param.15) | copy-start | bytes 6148
  0.0 3.2 %copy-start.3 = (s32[256,2]{0,1:T(2,128)S(1)}, s32[256,2]{0,1:T(2,128)}, u32[]{:S(2)}) copy-start(s32[256,2]{0,1:T(2,128)} %param.14) | copy-start | bytes 6148
  0.0 3.9 %copy-start.1 = (f32[2048]{0:T(1024)S(1)}, f32[2048]{0:T(1024)}, u32[]{:S(2)}) copy-start(f32[2048]{0:T(1024)} %param.10) | copy-start | bytes 24580
  0.0 3.9 %copy-start.2 = (f32[2048]{0:T(1024)S(1)}, f32[2048]{0:T(1024)}, u32[]{:S(2)}) copy-start(f32[2048]{0:T(1024)} %param.9) | copy-start | bytes 24580

commit v4 on v3

--- a/solution.py
+++ b/solution.py
@@ -14,15 +14,15 @@
 
 
 def kernel(
-    planes, nrm, meta, gw, uw, dw, out,
-    tok, met, wg, wu, wd, sel, mix, snd, xin, hid, res, ret, psend, racc,
+    planes, raw, gain, bias, meta, gw, uw, dw, out,
+    src, tok, met, wg, wu, wd, sel, mix, snd, xin, hid, res, ret, psend, racc,
     s_own, s_met, s_mets, s_wl, s_ws, s_wr, s_tok, s_toks, s_x, s_xs, s_r, s_rs, s_p, s_ps,
 ):
     n = LINE
     side = planes
     me, core = lax.axis_index("ep"), lax.axis_index("tp")
     z, p = me // side, lax.rem(me, side)
-    tokens, width = nrm.shape
+    tokens, width = raw.shape
     half = gw.shape[2]
     rows = snd.shape[1]
     cap = rows // side
@@ -61,7 +61,7 @@
         pltpu.make_async_copy(ref, ref, sem).wait()
 
     barrier = pltpu.get_barrier_semaphore()
-    own = pltpu.make_async_copy(nrm, tok.at[z], s_own.at[0])
+    own = pltpu.make_async_copy(raw, src, s_own.at[0])
     own.start()
     ownm = pltpu.make_async_copy(meta, met.at[z], s_own.at[1])
     ownm.start()
@@ -74,7 +74,6 @@
             barrier, inc=1, device_id=plane(lax.rem(z + j, n)), device_id_type=MESH
         )
     pl.semaphore_signal(barrier, inc=1, device_id={"tp": 1 - core}, device_id_type=MESH)
-    pl.semaphore_wait(barrier, side - 1 + n)
 
     def send_tok(s, c, to, way):
         remote(
@@ -86,25 +85,6 @@
         @pl.loop(0, k)
         def _(c):
             send_tok(z, c, to, way)
-
-    own.wait()
-    ownm.wait()
-    for j in range(1, n):
-        remote(
-            met.at[z], met.at[z], s_mets.at[j - 1], s_met.at[z], plane(lax.rem(z + j, n))
-        ).start()
-
-    @pl.when(end)
-    def _():
-        send_own(za, 0)
-
-    halfrows = pl.ds(pl.multiple_of(core * half, half), half)
-    pairs = [
-        (gw.at[0], wg.at[core]), (uw.at[0], wu.at[core]), (dw.at[0], wd.at[halfrows]),
-    ]
-    for i, (a, b) in enumerate(pairs):
-        pltpu.make_async_copy(a, b, s_wl.at[i]).start()
-        remote(a, b, s_ws.at[i], s_wr.at[i], {"tp": 1 - core}).start()
 
     def prep(q):
         s = order[q]
@@ -128,6 +108,38 @@
         mix[q, 0] = high
         mix[q, 1] = (w - high.astype(jnp.float32)).astype(jnp.bfloat16)
 
+    own.wait()
+    slab = min(32, tokens)
+
+    @pl.loop(0, tokens // slab)
+    def _(i):
+        at = pl.ds(pl.multiple_of(i * slab, slab), slab)
+        v = src[at, :].astype(jnp.float32)
+        v = v - jnp.mean(v, axis=-1, keepdims=True)
+        spread = jnp.mean(v * v, axis=-1, keepdims=True)
+        y = v * lax.rsqrt(spread + 1e-05) * gain[...] + bias[...]
+        tok[z, at, :] = y.astype(jnp.bfloat16)
+
+    ownm.wait()
+    prep(0)
+    pl.semaphore_wait(barrier, side - 1 + n)
+    for j in range(1, n):
+        remote(
+            met.at[z], met.at[z], s_mets.at[j - 1], s_met.at[z], plane(lax.rem(z + j, n))
+        ).start()
+
+    @pl.when(end)
+    def _():
+        send_own(za, 0)
+
+    halfrows = pl.ds(pl.multiple_of(core * half, half), half)
+    pairs = [
+        (gw.at[0], wg.at[core]), (uw.at[0], wu.at[core]), (dw.at[0], wd.at[halfrows]),
+    ]
+    for i, (a, b) in enumerate(pairs):
+        pltpu.make_async_copy(a, b, s_wl.at[i]).start()
+        remote(a, b, s_ws.at[i], s_wr.at[i], {"tp": 1 - core}).start()
+
     def disp(q, c):
         y = jnp.dot(sel[q], tok[order[q], :, cols(c)], preferred_element_type=jnp.float32)
         snd[q, :, cols(c)] = y.astype(jnp.bfloat16)
@@ -196,8 +208,6 @@
     def arrived(s, c):
         landed(tok.at[s, :, cols(c)], s_tok.at[s, c])
 
-    prep(0)
-
     @pl.loop(0, k)
     def _(c):
         disp(0, c)
@@ -207,38 +217,19 @@
         prep(q)
 
     def near(c):
-        @pl.when(mid)
-        def _():
-            arrived(order[2], c)
-            send_tok(order[2], c, za, 0)
-            disp(2, c)
+        arrived(order[2], c)
+        send_tok(order[2], c, za, 0)
+        disp(2, c)
 
     def far(c):
         arrived(order[1], c)
-
-        @pl.when(mid)
-        def _():
-            send_tok(order[1], c, zb, 1)
-
+        send_tok(order[1], c, zb, 1)
         disp(1, c)
 
-    for c in range(LAG):
-        near(c)
-
-    @pl.loop(LAG, k)
-    def _(c):
-        near(c)
-        far(c - LAG)
-
-    @pl.when(mid)
-    def _():
-        send_own(za, 0)
-
-    pl.loop(k - LAG, k)(far)
-
-    for i, (a, b) in enumerate(pairs):
-        pltpu.make_async_copy(a, b, s_wl.at[i]).wait()
-        landed(b, s_wr.at[i])
+    def weights():
+        for i, (a, b) in enumerate(pairs):
+            pltpu.make_async_copy(a, b, s_wl.at[i]).wait()
+            landed(b, s_wr.at[i])
 
     @pl.when(mid)
     def _():
@@ -247,6 +238,17 @@
             send_tok(order[3], c, zb, 1)
             disp(3, c)
 
+        for c in range(LAG):
+            near(c)
+
+        @pl.loop(LAG, k)
+        def _(c):
+            near(c)
+            far(c - LAG)
+
+        send_own(za, 0)
+        pl.loop(k - LAG, k)(far)
+        weights()
         pl.loop(0, k // 2)(pass_on)
         landed(others(xin, 1), s_x.at[1])
         turns = k - k // 2
@@ -272,6 +274,14 @@
 
     @pl.when(end)
     def _():
+        def take(c):
+            arrived(order[1], c)
+            disp(1, c)
+
+        pl.loop(0, k // 2)(take)
+        weights()
+        compute(0)
+        pl.loop(k // 2, k)(take)
         compute(1)
 
         @pl.loop(0, k)
@@ -280,7 +290,6 @@
             disp(2, c)
             combine(1, c, False)
 
-        compute(0)
         compute(2)
 
         @pl.loop(0, k)
@@ -337,23 +346,21 @@
     cap = max(4 * count // experts, 4)
     side = experts // LINE
     half = gate_weight.shape[2]
-    values = tokens.astype(jnp.float32)
-    centre = values - jnp.mean(values, axis=-1, keepdims=True)
-    spread = jnp.mean(centre * centre, axis=-1, keepdims=True)
-    normed = (centre * lax.rsqrt(spread + 1e-05) * norm_gain + norm_bias).astype(jnp.bfloat16)
     both = jnp.concatenate([expert_ids.astype(jnp.float32), route_weights], axis=1)
     meta = jnp.pad(both.T, ((0, 4), (0, 0)))
     rows = side * cap
     wide = width // CHUNKS
     bf = jnp.bfloat16
     dma = pltpu.SemaphoreType.DMA
+    vmem = pl.BlockSpec(memory_space=pltpu.VMEM)
     hbm = pl.BlockSpec(memory_space=pl.ANY)
     return pl.pallas_call(
         functools.partial(kernel, side),
         out_shape=jax.ShapeDtypeStruct((count, width), bf),
-        in_specs=[hbm] * 5,
+        in_specs=[hbm, vmem, vmem] + [hbm] * 4,
         out_specs=pl.BlockSpec(memory_space=pltpu.VMEM),
         scratch_shapes=[
+            pltpu.VMEM((count, width), bf),
             pltpu.VMEM((LINE, count, width), bf),
             pltpu.VMEM((LINE, 8, count), jnp.float32),
             pltpu.VMEM((2, width, half), bf),
@@ -386,7 +393,7 @@
         compiler_params=pltpu.CompilerParams(
             collective_id=0, has_side_effects=True, vmem_limit_bytes=60 * 1024 * 1024
         ),
-    )(normed, meta, gate_weight, up_weight, down_weight)
+    )(tokens, norm_gain[None], norm_bias[None], meta, gate_weight, up_weight, down_weight)
 
 
 def solution(mesh):

time: 141 us -> 135 us (0.957)
  other arithmetic: 4.63 us -> 1.37 us
  Pallas kernels: 132 us -> 129 us
    reduce_sum x2 -> x0, other arithmetic: 3.18 us -> none  [the longest x1 1.64 us: body(): spread = jnp.mean(centre * centre, axis=-1, keepdims=True)]
    pallas_call x1, Pallas kernels: 132 us -> 129 us  [body(): pl.pallas_call(functools.partial(kernel, side), out_shape=jax.ShapeDtypeS...]
    convert_element_type x1 -> x0, other arithmetic: 1.43 us -> none  [body(): (centre * lax.rsqrt(spread + 1e-05) * norm_gain + norm_bias).astype(jnp.b...]
where the time goes in v4:
time: 135 us; the launch traced here: 133 us
  Pallas kernels  129 us (96%)
  local copies, waits for them, and re-layouts  2.91 us (2%)
  other arithmetic  1.37 us (1%)
    pallas_call x1, Pallas kernels, body(): pl.pallas_call(functools.partial(kernel, side), out_shape=jax.ShapeDtypeS...  129 us

profile of v4, /device:TPU:14, one launch (start us, length us, event | category | flops | bytes accessed | tf_op | source)
XLA Modules:
  0.0 132.9 jit_solution(4084023963667462290)
XLA Ops:
  0.0 0.7 convert_element_type.5
  0.7 0.7 maximum_bitcast_fusion
  1.4 0.6 pad.4.meta
  2.0 128.6 %shard_map.82 = bf16[256,2048]{1,0:T(8,128)(2,1)} custom-call(bf16[256,2048]{1,0:T(8,128)(2,1)} %raw.1, f32[1,2048]{1,0:T(1,128)} %bitcast.4, f32[1,2048]{1,0:T(1,128)} %bitcast.5, f32[8,256]{1,0:T(8,128)} %pad.4.meta, bf16[1,2048,512]{2,1,0:T(8,128)(2,1)} %gw.1, bf16[1,2048,512]{2,1,0:T(8,128)(2,1)} %uw.1, bf16[1,512,2048]{2,1,0:T(8,128)(2,1)} %dw.1), custom_call_target="tpu_custom_call" | custom-call | tf_op jit(solution)/shard_map/pallas_call | solution.py:357
  130.6 2.3 %copy.10 = bf16[256,2048]{1,0:T(8,128)(2,1)} copy(bf16[256,2048]{1,0:T(8,128)(2,1)} %shard_map.82) | data formatting | bytes 2097152
